TPU v7x, 32 devices: a whole 2x2x4 slice. The times are simulated.
32 devices in a mesh: sp: 8 (over z, y), tp: 4 (over x, core).
Axes of the slice: x: 2, y: 2, z: 4, core: 2. Of those that a mesh axis runs over, the one named last changes fastest.
Arguments:
- queries: bfloat16 [8192, 1024], P('sp', 'tp'), may hold values from -6 to 6
- cell_key_rows: bfloat16 [8192, 1024], P('sp', 'tp'), may hold values from -6 to 6
- cell_value_rows: bfloat16 [8192, 2048], P('sp', 'tp'), may hold values from -6 to 6
- output_gate_logits: bfloat16 [8192, 2048], P('sp', 'tp'), may hold values from -6 to 6
- input_gate_logits: bfloat16 [8, 8192], P('tp', 'sp'), may hold values from -4 to 216
- forget_gate_logits: bfloat16 [8, 8192], P('tp', 'sp'), may hold values from 0.5 to 14
- forget_extra_term: float32 [8, 8192], P('tp', 'sp'), may hold values from -1.4 to 0
- residual: bfloat16 [8192, 2048], P('sp', 'tp'), may hold values from -13 to 13
- head_norm_gain: bfloat16 [2048], P('tp'), may hold values from 0.099609375 to 1.8984375
- cell_output_weight: bfloat16 [2048, 2048], P('tp'), may hold values from -0.25 to 0.25
- feedforward_norm_gain: bfloat16 [2048], replicated, may hold values from 0.099609375 to 1.8984375
- gate_projection_weight: bfloat16 [2048, 5632], P('sp', 'tp'), may hold values from -0.125 to 0.125
- up_projection_weight: bfloat16 [2048, 5632], P('sp', 'tp'), may hold values from -0.125 to 0.125
- down_projection_weight: bfloat16 [5632, 2048], P('tp', 'sp'), may hold values from -0.15625 to 0.15625
Outputs:
- mixed: bfloat16 [8192, 2048], P('sp', 'tp')
All inputs are finite; a program needn't handle non-finite values.
Results may differ from a plain program's by a relative error of at most 0.017.
Values may be sent and summed in bfloat16 or wider, within the bound.
A program may use at most 128 MiB of HBM per device.

v0:
```python
import jax
import jax.numpy as jnp
from jax import lax
from jax.sharding import PartitionSpec as P

PRECISE = lax.Precision.HIGHEST
LOWEST_LOG = -1e30
EPSILON = 1e-06


def entering(array, axis, combine, identity):
    length, index = (lax.axis_size(axis), lax.axis_index(axis))
    everything = jax.tree.map(lambda part: lax.all_gather(part, axis), array)
    start = jax.tree.map(
        lambda part, zero: jnp.broadcast_to(jnp.asarray(zero, part.dtype), part.shape),
        array,
        identity,
    )

    def step(k, before):
        reached = k < index
        new = combine(before, jax.tree.map(lambda part: part[k], everything))
        return jax.tree.map(lambda a, b: jnp.where(reached, a, b), new, before)

    return lax.fori_loop(0, length, step, start)


def to_blocks(array, block_count, block_size):
    shaped = array.reshape((array.shape[0], block_count, block_size) + array.shape[2:])
    return jnp.moveaxis(shaped, 1, 0)


def from_blocks(array):
    moved = jnp.moveaxis(array, 0, 1)
    return moved.reshape((moved.shape[0], moved.shape[1] * moved.shape[2]) + moved.shape[3:])


def memory_blocks(
    query_raw, key_raw, value_heads, in_gates, forget_log_value, block_size, query_scale
):
    head_count, length, key_width = query_raw.shape
    value_width = value_heads.shape[2]
    block_count = length // block_size
    causal = jnp.tril(jnp.ones((block_size, block_size), bool))

    def advance(carried, pieces):
        memory_state, top_log, offset = carried
        query_block, key_block, value_block, gate_block, forget_block = pieces
        running = jnp.cumsum(forget_block, axis=-1)
        log_weight = jnp.where(
            causal, running[:, :, None] - running[:, None, :] + gate_block[:, None, :], -jnp.inf
        )
        log_start = running + top_log[:, None]
        row_max = jnp.maximum(jnp.max(log_weight, axis=-1), log_start)
        scores = jnp.einsum(
            "htd,hsd->hts", query_block, key_block, preferred_element_type=jnp.float32
        )
        scores = scores * query_scale * jnp.exp(log_weight - row_max[:, :, None])
        query_wide = query_block.astype(jnp.float32) * query_scale
        earlier = jnp.einsum("htd,hde->hte", query_wide, memory_state, precision=PRECISE)
        numerator = jnp.exp(log_start - row_max)[:, :, None] * earlier
        numerator = numerator + jnp.einsum("hts,hse->hte", scores, value_block, precision=PRECISE)
        last_cum = running[:, -1]
        log_end = last_cum[:, None] - running + gate_block
        new_top = jnp.maximum(last_cum + top_log, jnp.max(log_end, axis=-1))
        scaled = key_block.astype(jnp.float32) * jnp.exp(log_end - new_top[:, None])[:, :, None]
        memory_state = jnp.exp(last_cum + top_log - new_top)[:, None, None] * memory_state
        memory_state = memory_state + jnp.einsum(
            "hsd,hse->hde", scaled, value_block, precision=PRECISE
        )
        return (
            (memory_state, new_top, offset + last_cum),
            (numerator, row_max, offset[:, None] + running),
        )

    initial = (
        jnp.zeros((head_count, key_width, value_width), jnp.float32),
        jnp.full((head_count,), LOWEST_LOG, jnp.float32),
        jnp.zeros((head_count,), jnp.float32),
    )
    pieces = tuple(
        (
            to_blocks(array, block_count, block_size)
            for array in (query_raw, key_raw, value_heads, in_gates, forget_log_value)
        )
    )
    ending, outputs = lax.scan(advance, initial, pieces)
    return (tuple((from_blocks(output) for output in outputs)), ending)


def join_states(earlier, later):
    state_early, top_early, total_early = earlier
    state_late, top_late, total_late = later
    moved_top = top_early + total_late
    new_top = jnp.maximum(moved_top, top_late)
    joined = jnp.exp(moved_top - new_top)[:, None, None] * state_early
    joined = joined + jnp.exp(top_late - new_top)[:, None, None] * state_late
    return (joined, new_top, total_early + total_late)


def heads_first(array, head_count):
    token_rows = array.shape[0]
    width = array.shape[1] // head_count
    return jnp.transpose(array.reshape(token_rows, head_count, width), (1, 0, 2))


def local(
    queries,
    cell_key_rows,
    cell_value_rows,
    output_gate_logits,
    input_gate_logits,
    forget_gate_logits,
    forget_extra_term,
    residual,
    head_norm_gain,
    cell_output_weight,
    feedforward_norm_gain,
    gate_projection_weight,
    up_projection_weight,
    down_projection_weight,
):
    whole_gate, whole_up, whole_down = (
        lax.all_gather(gate_projection_weight, "sp", axis=0, tiled=True),
        lax.all_gather(up_projection_weight, "sp", axis=0, tiled=True),
        lax.all_gather(down_projection_weight, "sp", axis=1, tiled=True),
    )
    token_rows = queries.shape[0]
    head_count = input_gate_logits.shape[0]
    key_width = queries.shape[1] // head_count
    value_width = cell_value_rows.shape[1] // head_count
    query_scale = key_width ** (-0.5)
    query_raw = heads_first(queries, head_count)
    key_raw = heads_first(cell_key_rows, head_count)
    value_heads = heads_first(cell_value_rows, head_count).astype(jnp.float32)
    forget_log_value = (
        jax.nn.log_sigmoid(forget_gate_logits.astype(jnp.float32)) + forget_extra_term
    )
    results, ending = memory_blocks(
        query_raw,
        key_raw,
        value_heads,
        input_gate_logits.astype(jnp.float32),
        forget_log_value,
        min(token_rows, 512),
        query_scale,
    )
    numerator, local_max, offsets = results
    end_state, end_top, end_total = ending
    identity = (
        jnp.zeros_like(end_state),
        jnp.full_like(end_top, LOWEST_LOG),
        jnp.zeros_like(end_total),
    )
    carried_state, carried_top, _ = entering(
        (end_state, end_top, end_total), "sp", join_states, identity
    )
    shifted = offsets + carried_top[:, None]
    row_max = jnp.maximum(local_max, shifted)
    query_heads = query_raw.astype(jnp.float32) * query_scale
    from_before = jnp.einsum("htd,hde->hte", query_heads, carried_state, precision=PRECISE)
    memory = (
        jnp.exp(local_max - row_max)[:, :, None] * numerator
        + jnp.exp(shifted - row_max)[:, :, None] * from_before
    )
    memory = jnp.transpose(memory, (1, 0, 2))
    normal = memory * lax.rsqrt(jnp.mean(memory * memory, axis=-1, keepdims=True) + EPSILON)
    gate_open = jax.nn.sigmoid(
        output_gate_logits.astype(jnp.float32).reshape(token_rows, head_count, value_width)
    )
    gated_heads = (
        normal * head_norm_gain.astype(jnp.float32).reshape(head_count, value_width) * gate_open
    )
    gated_heads = gated_heads.reshape(token_rows, head_count * value_width).astype(jnp.bfloat16)
    partial_value = jnp.dot(
        gated_heads, cell_output_weight, preferred_element_type=jnp.float32
    ).astype(jnp.bfloat16)
    column_count = residual.shape[1]
    column_start = lax.axis_index("tp") * column_count
    summed = lax.psum_scatter(partial_value, "tp", scatter_dimension=1, tiled=True).astype(
        jnp.float32
    )
    stream = (residual.astype(jnp.float32) + summed).astype(jnp.bfloat16)
    stream_local = stream.astype(jnp.float32)
    squares = lax.psum(jnp.sum(stream_local * stream_local, axis=1), "tp")
    scale = lax.rsqrt(squares / feedforward_norm_gain.shape[0] + EPSILON)[:, None]
    gain_columns = lax.dynamic_slice_in_dim(
        feedforward_norm_gain, column_start, column_count, 0
    ).astype(jnp.float32)
    normed = lax.all_gather(
        (stream_local * scale * gain_columns).astype(jnp.bfloat16), "tp", axis=1, tiled=True
    )
    gate_value = jnp.dot(normed, whole_gate, preferred_element_type=jnp.float32)
    lifted = jnp.dot(normed, whole_up, preferred_element_type=jnp.float32)
    hidden = (jax.nn.silu(gate_value) * lifted).astype(jnp.bfloat16)
    down_terms = jnp.dot(hidden, whole_down, preferred_element_type=jnp.float32)
    channel_total = lax.psum_scatter(
        down_terms.astype(jnp.bfloat16), "tp", scatter_dimension=1, tiled=True
    ).astype(jnp.float32)
    return (stream.astype(jnp.float32) + 0.5 * channel_total).astype(jnp.bfloat16)


def solution(mesh):
    placed = (
        P("sp", "tp"),
        P("sp", "tp"),
        P("sp", "tp"),
        P("sp", "tp"),
        P("tp", "sp"),
        P("tp", "sp"),
        P("tp", "sp"),
        P("sp", "tp"),
        P("tp"),
        P("tp", None),
        P(),
        P("sp", "tp"),
        P("sp", "tp"),
        P("tp", "sp"),
    )
    return jax.shard_map(
        local, mesh=mesh, in_specs=placed, out_specs=P("sp", "tp"), check_vma=False
    )
```

profile of v0, /device:TPU:0, one launch (start us, length us, event | category | flops | bytes accessed | tf_op | source)
XLA Modules:
  0.0 540.1 jit_solution(7199471552716918428)
XLA Ops:
  6.6 1.4 copy.44
  8.0 1.0 copy.45
  9.0 2.3 copy.42
  11.2 2.8 convert_bitcast_fusion
  14.1 2.9 copy.43
  17.0 1.3 copy.40
  18.6 18.4 %while.37 = (s32[]{:T(128)}, f32[2,128,256]{2,1,0:T(8,128)S(1)}, f32[2]{0:T(128)S(1)}, f32[2]{0:T(128)S(1)}, f32[2,2,512,256]{3,2,1,0:T(8,128)}, /*index=5*/f32[...) while((s32[]{:T(128)}, f32[2,128,256]{2,1,0:T(8,128)S(1)}, ...), condition=%wide.region_5.6_spmd.clone, body=%wide.region_0.5_spmd.clone.sunk | while | flops 2557093888 | bytes 39478384 | solution.py:87
  21.0 1.5 fusion.120
  22.5 2.6 fusion.122
  25.2 1.1 fusion.123
  26.4 1.3 convolution_add_fusion.2
  29.4 0.7 fusion.121
  30.1 1.5 fusion.120
  31.7 2.6 fusion.122
  34.4 1.1 fusion.123
  35.6 1.3 convolution_add_fusion.2
  37.0 0.7 copy-done.2
  39.5 23.3 %all-reduce.2 = (f32[16]{0:T(128)S(1)}, f32[16]{0:T(128)S(1)}) all-reduce(f32[16]{0:T(128)S(1)} %dynamic-update-slice, f32[16]{0:T(128)S(1)} %dynamic-update-slice.1), channel_id=2, replica_groups=mesh['sp'=8,'tp'=4] {'sp'}, use_global_device_ids=true, to_apply=%add | all-reduce | flops 32 | bytes 256
  63.0 4.2 copy.49
  67.1 4.2 reshape.321
  71.3 1.9 add_divide_fusion
  73.2 2.9 copy.52
  76.1 13.6 %all-gather.17.cloned.1.call-done = f32[16,128,256]{2,1,0:T(8,128)} async-done(((f32[2,128,256]{2,1,0:T(8,128)}), f32[16,128,256]{2,1,0:T(8,128)}) %all-gather.17.cloned.1.call-update) | async-done | bytes 2097168 | tf_op jit(solution)/shard_map/all_gather | solution.py:13
  89.8 9.1 %while.38 = (s32[]{:T(128)}, f32[2,128,256]{2,1,0:T(8,128)S(1)}, f32[2]{0:T(128)S(1)}, s32[]{:T(128)}, f32[8,2]{1,0:T(8,128)S(1)}, /*index=5*/f32[8,2]{1,0:T(8,1...) while((s32[]{:T(128)}, f32[2,128,256]{2,1,0:T(8,128)S(1)}, f32[2]{0:T(128)S(1)}, s32[]{:T(128)}, ...), condition=%wide.region_7.8_spmd.clone, body=%wide.region_6.7_spmd.clone.sunk | while | flops 327698 | bytes 786647 | solution.py:25
  89.8 1.1 fusion.124
  91.0 1.1 fusion.124
  92.1 1.1 fusion.124
  93.3 1.1 fusion.124
  94.4 1.1 fusion.124
  95.5 1.1 fusion.124
  96.6 1.1 fusion.124
  97.8 1.1 fusion.124
  99.0 3.9 fusion.58
  103.2 4.4 convolution_convert_fusion.1
  107.7 0.7 all-gather.11.cloned.1.call-update
  108.5 0.8 dynamic-slice_convert_fusion
  109.2 41.6 %reduce-scatter.3.cloned.1.call-done = bf16[1024,512]{1,0:T(8,128)(2,1)} async-done(((bf16[1024,2048]{1,0:T(8,128)(2,1)}), bf16[1024,512]{1,0:T(8,128)(2,1)}) %reduce-scatter.3.cloned.1.call-update) | async-done | bytes 1048592 | tf_op jit(solution)/shard_map/reduce_scatter | solution.py:180
  150.8 1.7 fusion.54
  152.5 5.8 %psum.7 = f32[1024]{0:T(1024)S(1)} all-reduce(f32[1024]{0:T(1024)S(1)} %fusion.54), channel_id=1, replica_groups=mesh['sp'=8,'tp'=4] {'tp'}, use_global_device_ids=true, to_apply=%region_11.12 | all-reduce | flops 1024 | bytes 8192 | tf_op jit(solution)/shard_map/psum | solution.py:185
  158.3 1.4 fusion.56
  161.1 84.2 %all-gather.11.cloned.1.call-done = bf16[2048,1408]{1,0:T(8,128)(2,1)} async-done(((bf16[256,1408]{1,0:T(8,128)(2,1)}), bf16[2048,1408]{1,0:T(8,128)(2,1)}) %all-gather.11.cloned.1.call-update) | async-done | bytes 5767184 | tf_op jit(solution)/shard_map/all_gather | solution.py:124
  245.3 34.1 %all-gather.9.cloned.1.call-done = bf16[1024,2048]{1,0:T(8,128)(2,1)} async-done(((bf16[1024,512]{1,0:T(8,128)(2,1)}), bf16[1024,2048]{1,0:T(8,128)(2,1)}) %all-gather.9.cloned.1.call-update) | async-done | bytes 4194320 | tf_op jit(solution)/shard_map/all_gather | solution.py:190
  279.4 11.7 %fusion.74 = f32[1024,1408]{1,0:T(8,128)} fusion(bf16[1024,2048]{1,0:T(8,128)(2,1)} %all-gather.9.cloned.1.call-done, bf16[2048,1408]{1,0:T(8,128)(2,1)} %all-gather.11.cloned.1.call-done), kind=kOutput, calls=%fused_computation.117 | convolution fusion | flops 5905580032 | bytes 15728640 | tf_op jit(solution)/shard_map/dot_general | solution.py:193
  291.1 82.7 %all-gather.13.cloned.1.call-done = bf16[2048,1408]{1,0:T(8,128)(2,1)} async-done(((bf16[256,1408]{1,0:T(8,128)(2,1)}), bf16[2048,1408]{1,0:T(8,128)(2,1)}) %all-gather.13.cloned.1.call-update) | async-done | bytes 5767184 | tf_op jit(solution)/shard_map/all_gather | solution.py:125
  373.8 93.2 %all-gather.15.cloned.1.call-done = bf16[1408,2048]{1,0:T(8,128)(2,1)} async-done(((bf16[1408,256]{1,0:T(8,128)(2,1)}), bf16[1408,2048]{1,0:T(8,128)(2,1)}) %all-gather.15.cloned.1.call-update) | async-done | bytes 5767184 | tf_op jit(solution)/shard_map/all_gather | solution.py:126
  467.0 20.6 %convolution_convert_fusion = bf16[1024,2048]{1,0:T(8,128)(2,1)} fusion(bf16[1408,2048]{1,0:T(8,128)(2,1)} %all-gather.15.cloned.1.call-done, f32[1024,1408]{1,0:T(8,128)} %fusion.74, bf16[1024,2048]{1,0:T(8,128)(2,1)} %all-gather.9.cloned.1.call-done, bf16[2048,1408]{1,0:T(8,128)(2,1)} %all-gather.13.cloned.1.call-done), kind=kOutput, calls=%fused_computation.80 | convolution fusion | flops 11821907968 | bytes 25690112 | tf_op jit(solution)/shard_map/dot_general | solution.py:196
  487.6 42.7 %reduce-scatter.5.cloned.1.call-done = bf16[1024,512]{1,0:T(8,128)(2,1)} async-done(((bf16[1024,2048]{1,0:T(8,128)(2,1)}), bf16[1024,512]{1,0:T(8,128)(2,1)}) %reduce-scatter.5.cloned.1.call-update) | async-done | bytes 1048592 | tf_op jit(solution)/shard_map/reduce_scatter | solution.py:197
  530.3 3.0 fusion.57
  (130 shorter events, 8.4 us)
Async XLA Ops:
  6.5 96.7 %copy-start = (bf16[512,2048]{1,0:T(8,128)(2,1)S(1)}, bf16[512,2048]{1,0:T(8,128)(2,1)}, u32[]{:S(2)}) copy-start(bf16[512,2048]{1,0:T(8,128)(2,1)} %param.27) | copy-start | bytes 6291460
  6.5 83.2 %all-gather.17.cloned.1.call-start = ((), (), s32[]{:S(2)}) async-start(), calls=%async_computation.8 | async-start | bytes 2359296 | tf_op jit(solution)/shard_map/all_gather | solution.py:13
  8.0 6.1 %copy-start.8 = (bf16[1024,256]{0,1:T(8,128)(2,1)}, bf16[1024,256]{0,1:T(8,128)(2,1)S(1)}, u32[]{:S(2)}) copy-start(bf16[1024,256]{0,1:T(8,128)(2,1)S(1)} %copy.44) | copy-start | bytes 1572868
  17.0 1.6 copy-start.14
  17.0 1.6 copy-start.13
  17.0 1.6 copy-start.15
  18.6 19.2 %copy-start.17 = (u32[32]{0:T(128)S(1)}, u32[32]{0:T(128)}, u32[]{:S(2)}) copy-start(u32[32]{0:T(128)} %constant.100) | copy-start | bytes 388
  20.8 1.7 copy-start.3
  22.5 2.7 copy-start.4
  22.5 2.7 copy-start.10
  26.3 1.4 copy-start.11
  30.0 1.7 copy-start.3
  31.7 2.7 copy-start.4
  31.7 2.7 copy-start.10
  35.5 1.4 copy-start.11
  37.0 0.7 copy-start.2
  37.8 113.0 %reduce-scatter.3.cloned.1.call-start = ((), (), s32[]{:S(2)}) async-start(), calls=%async_computation.2 | async-start | bytes 5242880 | tf_op jit(solution)/shard_map/reduce_scatter | solution.py:180
  67.1 4.2 copy-start.12
  73.2 2.9 copy-start.16
  89.8 9.2 %copy-start.9 = (bf16[1024,256]{0,1:T(8,128)(2,1)S(1)}, bf16[1024,256]{0,1:T(8,128)(2,1)}, u32[]{:S(2)}) copy-start(bf16[1024,256]{0,1:T(8,128)(2,1)} %copy-done.8) | copy-start | bytes 1572868
  99.0 3.9 copy-start.7
  107.6 43.1 %copy-start.5 = (bf16[1024,512]{1,0:T(8,128)(2,1)S(1)}, bf16[1024,512]{1,0:T(8,128)(2,1)}, u32[]{:S(2)}) copy-start(bf16[1024,512]{1,0:T(8,128)(2,1)} %param.25) | copy-start | bytes 3145732
  107.7 137.6 %all-gather.11.cloned.1.call-start = ((), (), s32[]{:S(2)}) async-start(), calls=%async_computation.4 | async-start | bytes 6488064 | tf_op jit(solution)/shard_map/all_gather | solution.py:124
  108.4 171.0 %all-gather.9.cloned.1.call-start = ((), (), s32[]{:S(2)}) async-start(), calls=%async_computation.3 | async-start | bytes 5242880 | tf_op jit(solution)/shard_map/all_gather | solution.py:190
  150.8 7.5 %copy-start.6 = (bf16[1024,512]{1,0:T(8,128)(2,1)S(1)}, bf16[1024,512]{1,0:T(8,128)(2,1)}, u32[]{:S(2)}) copy-start(bf16[1024,512]{1,0:T(8,128)(2,1)} %reduce-scatter.3.cloned.1.call-done) | copy-start | bytes 3145732
  159.7 214.1 %all-gather.13.cloned.1.call-start = ((), (), s32[]{:S(2)}) async-start(), calls=%async_computation.5 | async-start | bytes 6488064 | tf_op jit(solution)/shard_map/all_gather | solution.py:125
  160.3 306.7 %all-gather.15.cloned.1.call-start = ((), (), s32[]{:S(2)}) async-start(), calls=%async_computation.6 | async-start | bytes 6488064 | tf_op jit(solution)/shard_map/all_gather | solution.py:126
  160.9 369.5 %reduce-scatter.5.cloned.1.call-start = ((), (), s32[]{:S(2)}) async-start(), calls=%async_computation.7 | async-start | bytes 5242880 | tf_op jit(solution)/shard_map/reduce_scatter | solution.py:197
  487.6 45.7 %copy-start.1 = (bf16[512,2048]{1,0:T(8,128)(2,1)S(1)}, bf16[512,2048]{1,0:T(8,128)(2,1)}, u32[]{:S(2)}) copy-start(bf16[512,2048]{1,0:T(8,128)(2,1)} %param.27) | copy-start | bytes 6291460
Sparse Core Ops, SparseCore 0:
  37.9 51.8 all-gather.16
  107.8 42.9 reduce-scatter.2
  153.0 92.2 all-gather.10
  246.7 32.6 all-gather.8
  281.4 92.3 all-gather.12
  375.7 91.3 all-gather.14
  487.7 42.5 reduce-scatter.4
where the time goes:
time: 541 us; the launch traced here: 540 us
  waiting for transfers between devices  394 us (73%)
  matrix products  53.6 us (10%)
  blocking collectives  29.1 us (5%)
  other arithmetic  25.1 us (5%)
  local copies, waits for them, and re-layouts  23.3 us (4%)
  between operations  14.3 us (3%)
    all_gather x1, waiting for transfers between devices, local(): lax.all_gather(down_projection_weight, 'sp', axis=1, tiled=True)  93.2 us
    all_gather x1, waiting for transfers between devices, local(): lax.all_gather(gate_projection_weight, 'sp', axis=0, tiled=True)  84.2 us
    all_gather x1, waiting for transfers between devices, local(): lax.all_gather(up_projection_weight, 'sp', axis=0, tiled=True)  82.7 us
    reduce_scatter x1, waiting for transfers between devices, local(): lax.psum_scatter(down_terms.astype(jnp.bfloat16), 'tp', scatter_dimension...  42.7 us
    reduce_scatter x1, waiting for transfers between devices, local(): lax.psum_scatter(partial_value, 'tp', scatter_dimension=1, tiled=True)  41.6 us
    all_gather x1, waiting for transfers between devices, local(): lax.all_gather((stream_local * scale * gain_columns).astype(jnp.bfloat16)...  34.1 us
    unnamed x1, blocking collectives  23.3 us
    dot_general x1, matrix products, local(): down_terms = jnp.dot(hidden, whole_down, preferred_element_type=jnp.float32)  20.6 us
  transfers between devices with their start and end apart: 7, of which 7 were waited for; matrix products, arithmetic and copies ran while one was open for 6% of the time, Pallas kernels for 0%

commit v1 on v0

v1 whole, which is shorter than its diff:
```python
import jax
import jax.numpy as jnp
from jax import lax
from jax.experimental import pallas as pl
from jax.experimental.pallas import tpu as pltpu
from jax.sharding import PartitionSpec as P

LOWEST_LOG = -1e30
EPSILON = 1e-06


def shift_pairs(length, step):
    return [(source, source + step) for source in range(length - step)]


def entering_state(state, top, total):
    length, index = lax.axis_size("sp"), lax.axis_index("sp")
    heads, key_width, value_width = state.shape

    def pack(s, t, f):
        tail = jnp.zeros((heads, 8, value_width), jnp.float32)
        tail = tail.at[:, 0, :].set(t[:, None]).at[:, 1, :].set(f[:, None])
        return jnp.concatenate([s, tail], axis=1)

    def unpack(p, valid):
        s = p[:, :key_width, :]
        t = jnp.where(valid, p[:, key_width, 0], LOWEST_LOG)
        f = jnp.where(valid, p[:, key_width + 1, 0], 0.0)
        return jnp.where(valid, s, 0.0), t, f

    moved = lax.ppermute(pack(state, top, total), "sp", shift_pairs(length, 1))
    s, t, f = unpack(moved, index >= 1)
    step = 1
    while step < length - 1:
        moved = lax.ppermute(pack(s, t, f), "sp", shift_pairs(length, step))
        s0, t0, f0 = unpack(moved, index >= step)
        from_top = t0 + f
        new_top = jnp.maximum(from_top, t)
        s = (
            jnp.exp(from_top - new_top)[:, None, None] * s0
            + jnp.exp(t - new_top)[:, None, None] * s
        )
        t, f = new_top, f0 + f
        step *= 2
    return s, t


def cell_kernel(q_ref, k_ref, v_ref, a_ref, m_ref, c_ref, state_ref, open_ref, gain_ref, o_ref, *, scale):
    block = q_ref.shape[0]
    length = k_ref.shape[0]
    q = q_ref[...]
    first = pl.program_id(1) * block
    scores = lax.dot_general(
        q, k_ref[...], (((1,), (1,)), ((), ())), preferred_element_type=jnp.float32
    )
    rows = first + lax.broadcasted_iota(jnp.int32, (block, length), 0)
    cols = lax.broadcasted_iota(jnp.int32, (block, length), 1)
    weight = jnp.where(cols <= rows, jnp.exp(jnp.minimum(a_ref[0] - m_ref[0], 0.0)), 0.0)
    numer = jnp.dot(
        (scores * weight).astype(jnp.bfloat16), v_ref[...], preferred_element_type=jnp.float32
    )
    before = jnp.dot(q, state_ref[0].astype(jnp.bfloat16), preferred_element_type=jnp.float32)
    memory = (numer + c_ref[0] * before) * scale
    normal = memory * lax.rsqrt(jnp.mean(memory * memory, axis=-1, keepdims=True) + EPSILON)
    gate_open = jax.nn.sigmoid(open_ref[...].astype(jnp.float32))
    o_ref[...] = (normal * gain_ref[...].astype(jnp.float32) * gate_open).astype(o_ref.dtype)


def cell(queries, keys, values, a_log, m_col, c_col, state, open_logits, gain):
    heads, length = a_log.shape
    dk, dv = queries.shape[1] // heads, values.shape[1] // heads
    block = min(length, 256)
    return pl.pallas_call(
        lambda *refs: cell_kernel(*refs, scale=dk ** (-0.5)),
        grid=(heads, length // block),
        in_specs=[
            pl.BlockSpec((block, dk), lambda h, i: (i, h)),
            pl.BlockSpec((length, dk), lambda h, i: (0, h)),
            pl.BlockSpec((length, dv), lambda h, i: (0, h)),
            pl.BlockSpec((1, 1, length), lambda h, i: (h, 0, 0)),
            pl.BlockSpec((1, block, 1), lambda h, i: (h, i, 0)),
            pl.BlockSpec((1, block, 1), lambda h, i: (h, i, 0)),
            pl.BlockSpec((1, dk, dv), lambda h, i: (h, 0, 0)),
            pl.BlockSpec((block, dv), lambda h, i: (i, h)),
            pl.BlockSpec((1, dv), lambda h, i: (0, h)),
        ],
        out_specs=pl.BlockSpec((block, dv), lambda h, i: (i, h)),
        out_shape=jax.ShapeDtypeStruct((length, heads * dv), jnp.bfloat16),
        cost_estimate=pl.CostEstimate(
            flops=8 * heads * length * length * dv, bytes_accessed=6 * length * heads * dv, transcendentals=0
        ),
        name="cell",
    )(queries, keys, values, a_log[:, None, :], m_col[:, :, None], c_col[:, :, None], state, open_logits, gain)


def partner_pairs(count):
    return [(i, i ^ 1) for i in range(count)]


def ring_pairs(count, step):
    return [(i, (i + 2 * step) % count) for i in range(count)]


def take(array, index):
    return lax.dynamic_index_in_dim(array, index, 1, keepdims=False)


def product_scattered(rows, weight):
    count, index = lax.axis_size("tp"), lax.axis_index("tp")
    chips, core, chip = count // 2, index % 2, index // 2
    width = weight.shape[1] // count
    split = weight.reshape(weight.shape[0], chips, 2, width)

    def half(which):
        chosen = lax.dynamic_index_in_dim(split, which, 2, keepdims=False)
        return jnp.dot(
            rows, chosen.reshape(weight.shape[0], chips * width), preferred_element_type=jnp.float32
        )

    given = half(1 - core).astype(jnp.bfloat16)
    got = lax.ppermute(given, "tp", partner_pairs(count))
    kept = half(core).astype(jnp.bfloat16)
    shape = (rows.shape[0], chips, width)
    kept, got = kept.reshape(shape), got.reshape(shape)
    total = take(kept, chip).astype(jnp.float32) + take(got, chip).astype(jnp.float32)
    for step in range(1, chips):
        to = (chip + step) % chips
        sent = take(kept, to).astype(jnp.float32) + take(got, to).astype(jnp.float32)
        total = total + lax.ppermute(
            sent.astype(jnp.bfloat16), "tp", ring_pairs(count, step)
        ).astype(jnp.float32)
    return total


def columns_gathered(block):
    count, index = lax.axis_size("tp"), lax.axis_index("tp")
    chips, core, chip = count // 2, index % 2, index // 2
    width = block.shape[1]
    whole = jnp.zeros((block.shape[0], count * width), block.dtype)
    held = [(chip, block)]
    for step in range(1, chips):
        moved = lax.ppermute(block, "tp", ring_pairs(count, step))
        held.append(((chip - step) % chips, moved))
    for place, piece in held:
        other = lax.ppermute(piece, "tp", partner_pairs(count))
        whole = lax.dynamic_update_slice(whole, piece, (0, (2 * place + core) * width))
        whole = lax.dynamic_update_slice(whole, other, (0, (2 * place + 1 - core) * width))
    return whole


def local(
    queries,
    cell_key_rows,
    cell_value_rows,
    output_gate_logits,
    input_gate_logits,
    forget_gate_logits,
    forget_extra_term,
    residual,
    head_norm_gain,
    cell_output_weight,
    feedforward_norm_gain,
    gate_projection_weight,
    up_projection_weight,
    down_projection_weight,
):
    whole_gate = lax.all_gather(gate_projection_weight, "sp", axis=0, tiled=True)
    whole_up = lax.all_gather(up_projection_weight, "sp", axis=0, tiled=True)
    whole_down = lax.all_gather(down_projection_weight, "sp", axis=1, tiled=True)
    length = queries.shape[0]
    heads = input_gate_logits.shape[0]
    dk, dv = queries.shape[1] // heads, cell_value_rows.shape[1] // heads
    log_forget = jax.nn.log_sigmoid(forget_gate_logits.astype(jnp.float32)) + forget_extra_term
    running = jnp.cumsum(log_forget, axis=-1)
    a_log = input_gate_logits.astype(jnp.float32) - running
    m_log = lax.cummax(a_log, axis=1)
    a_top, total = m_log[:, -1], running[:, -1]
    decay = jnp.exp(a_log - a_top[:, None])
    weighed = (
        cell_key_rows.reshape(length, heads, dk).astype(jnp.float32) * decay.T[:, :, None]
    ).astype(jnp.bfloat16)
    state = jnp.stack(
        [
            lax.dot_general(
                weighed[:, h],
                cell_value_rows[:, h * dv : (h + 1) * dv],
                (((0,), (0,)), ((), ())),
                preferred_element_type=jnp.float32,
            )
            for h in range(heads)
        ]
    )
    carried, carried_top = entering_state(state, a_top + total, total)
    m_all = jnp.maximum(m_log, carried_top[:, None])
    coefficient = jnp.exp(carried_top[:, None] - m_all)
    gated = cell(
        queries,
        cell_key_rows,
        cell_value_rows,
        a_log,
        m_all,
        coefficient,
        carried,
        output_gate_logits,
        head_norm_gain[None, :],
    )
    summed = product_scattered(gated, cell_output_weight)
    stream = (residual.astype(jnp.float32) + summed).astype(jnp.bfloat16)
    wide = columns_gathered(stream).astype(jnp.float32)
    scale = lax.rsqrt(jnp.mean(wide * wide, axis=-1, keepdims=True) + EPSILON)
    normed = (wide * scale * feedforward_norm_gain.astype(jnp.float32)[None, :]).astype(jnp.bfloat16)
    gate_value = jnp.dot(normed, whole_gate, preferred_element_type=jnp.float32)
    lifted = jnp.dot(normed, whole_up, preferred_element_type=jnp.float32)
    hidden = (jax.nn.silu(gate_value) * lifted).astype(jnp.bfloat16)
    channel_total = product_scattered(hidden, whole_down)
    return (stream.astype(jnp.float32) + 0.5 * channel_total).astype(jnp.bfloat16)


def solution(mesh):
    placed = (
        P("sp", "tp"),
        P("sp", "tp"),
        P("sp", "tp"),
        P("sp", "tp"),
        P("tp", "sp"),
        P("tp", "sp"),
        P("tp", "sp"),
        P("sp", "tp"),
        P("tp"),
        P("tp", None),
        P(),
        P("sp", "tp"),
        P("sp", "tp"),
        P("tp", "sp"),
    )
    return jax.shard_map(
        local, mesh=mesh, in_specs=placed, out_specs=P("sp", "tp"), check_vma=False
    )
```

time: 541 us -> 380 us (0.70)
  waiting for transfers between devices: 394 us -> 192 us
  starting transfers between devices: 0.46 us -> 60 us
  blocking collectives: 29.1 us -> 0 us
  local copies, waits for them, and re-layouts: 23.3 us -> 45.9 us
  matrix products: 53.6 us -> 37.6 us
  Pallas kernels: 0 us -> 9.19 us
    all_gather x1, waiting for transfers between devices: 93.2 us -> 0.02 us  [local(): lax.all_gather(down_projection_weight, 'sp', axis=1, tiled=True)]
    ppermute x0 -> x11, waiting for transfers between devices: none -> 93 us  [the longest x2 46.1 us: product_scattered(): lax.ppermute(sent.astype(jnp.bfloat16), 'tp', ring_pairs(count, step))]
    reduce_scatter x2 -> x0, waiting for transfers between devices: 84.3 us -> none  [the longest x1 42.7 us: local(): lax.psum_scatter(down_terms.astype(jnp.bfloat16), 'tp', scatter_dimension...]
    all_gather x1, waiting for transfers between devices: 84.2 us -> 17.9 us  [local(): lax.all_gather(gate_projection_weight, 'sp', axis=0, tiled=True)]
    ppermute x0 -> x11, starting transfers between devices: none -> 59.9 us  [the longest x3 51.2 us: entering_state(): moved = lax.ppermute(pack(s, t, f), 'sp', shift_pairs(length, step))]
    all_gather x3 -> x1, waiting for transfers between devices: 130 us -> 80.7 us  [local(): whole_up = lax.all_gather(up_projection_weight, 'sp', axis=0, tiled=True)]
    unnamed x1 -> x0, blocking collectives: 23.3 us -> none
    dynamic_slice x2 -> x6, local copies, waits for them, and re-layouts: 0.01 us -> 18 us  [the longest x4 11.7 us: take(): return lax.dynamic_index_in_dim(array, index, 1, keepdims=False)]
  transfers between devices with their start and end apart: 7 -> 14, of which waited for: 7 -> 10; matrix products, arithmetic and copies ran while one was open for 6% -> 19% of each run, Pallas kernels for 0% -> 2%
where the time goes in v1:
time: 380 us; the launch traced here: 379 us
  waiting for transfers between devices  192 us (51%)
  starting transfers between devices  60 us (16%)
  local copies, waits for them, and re-layouts  45.9 us (12%)
  matrix products  37.6 us (10%)
  other arithmetic  20.3 us (5%)
  between operations  13.6 us (4%)
  Pallas kernels  9.19 us (2%)
    all_gather x1, waiting for transfers between devices, local(): whole_up = lax.all_gather(up_projection_weight, 'sp', axis=0, tiled=True)  80.7 us
    ppermute x3, starting transfers between devices, entering_state(): moved = lax.ppermute(pack(s, t, f), 'sp', shift_pairs(length, step))  51.2 us
    ppermute x2, waiting for transfers between devices, product_scattered(): lax.ppermute(sent.astype(jnp.bfloat16), 'tp', ring_pairs(count, step))  46.1 us
    ppermute x1, waiting for transfers between devices, columns_gathered(): moved = lax.ppermute(block, 'tp', ring_pairs(count, step))  23.2 us
    all_gather x1, waiting for transfers between devices, local(): lax.all_gather(gate_projection_weight, 'sp', axis=0, tiled=True)  17.9 us
    dot_general x4, matrix products, half(): jnp.dot(rows, chosen.reshape(weight.shape[0], chips * width), preferred_e...  13.7 us
    dot_general x1, matrix products, local(): gate_value = jnp.dot(normed, whole_gate, preferred_element_type=jnp.float32)  12 us
    ppermute x3, waiting for transfers between devices, entering_state(): moved = lax.ppermute(pack(s, t, f), 'sp', shift_pairs(length, step))  11.8 us
  transfers between devices with their start and end apart: 14, of which 10 were waited for; matrix products, arithmetic and copies ran while one was open for 19% of the time, Pallas kernels for 2%

profile of v1, /device:TPU:0, one launch (start us, length us, event | category | flops | bytes accessed | tf_op | source)
XLA Modules:
  0.0 378.8 jit_solution(3015606708128410608)
XLA Ops:
  6.6 2.4 copy.58
  13.3 4.9 %collective-permute-start = (f32[2,136,256]{2,1,0:T(8,128)S(1)}, f32[2,136,256]{2,1,0:T(8,128)S(1)}, u32[]{:S(2)}, u32[]{:S(2)}) collective-permute-start(f32[2,136,256]{2,1,0:T(8,128)S(1)} %pad_maximum_fusion), channel_id=1, source_target_pairs={{0,4},{4,8},{8,12},{12,16},{16,20},{20,24},{24,28},{1,5},{5,9},{9,... | collective-permute-start | bytes 835592 | tf_op jit(solution)/shard_map/ppermute | solution.py:31
  18.3 10.1 %collective-permute-done = f32[2,136,256]{2,1,0:T(8,128)S(1)} collective-permute-done((f32[2,136,256]{2,1,0:T(8,128)S(1)}, f32[2,136,256]{2,1,0:T(8,128)S(1)}, u32[]{:S(2)}, u32[]{:S(2)}) %collective-permute-start) | collective-permute-done | bytes 278560 | tf_op jit(solution)/shard_map/ppermute | solution.py:31
  28.8 4.4 %collective-permute-start.1 = (f32[2,136,256]{2,1,0:T(8,128)S(1)}, f32[2,136,256]{2,1,0:T(8,128)S(1)}, u32[]{:S(2)}, u32[]{:S(2)}) collective-permute-start(f32[2,136,256]{2,1,0:T(8,128)S(1)} %pad_maximum_fusion.1), channel_id=1, source_target_pairs={{0,4},{4,8},{8,12},{12,16},{16,20},{20,24},{24,28},{1,5},{5,9},{9,... | collective-permute-start | bytes 835592 | tf_op jit(solution)/shard_map/ppermute | solution.py:35
  33.2 4.6 %collective-permute-done.1 = f32[2,136,256]{2,1,0:T(8,128)S(1)} collective-permute-done((f32[2,136,256]{2,1,0:T(8,128)S(1)}, f32[2,136,256]{2,1,0:T(8,128)S(1)}, u32[]{:S(2)}, u32[]{:S(2)}) %collective-permute-start.1) | collective-permute-done | bytes 278560 | tf_op jit(solution)/shard_map/ppermute | solution.py:35
  38.3 12.6 %collective-permute-start.2 = (f32[2,136,256]{2,1,0:T(8,128)S(1)}, f32[2,136,256]{2,1,0:T(8,128)S(1)}, u32[]{:S(2)}, u32[]{:S(2)}) collective-permute-start(f32[2,136,256]{2,1,0:T(8,128)S(1)} %pad_maximum_fusion.2), channel_id=1, source_target_pairs={{0,8},{4,12},{8,16},{12,20},{16,24},{20,28},{1,9},{5,13},{9,17},{1... | collective-permute-start | bytes 835592 | tf_op jit(solution)/shard_map/ppermute | solution.py:35
  51.5 3.4 collective-permute-done.2
  56.2 34.2 %collective-permute-start.3 = (f32[2,136,256]{2,1,0:T(8,128)}, f32[2,136,256]{2,1,0:T(8,128)}, u32[]{:S(2)}, u32[]{:S(2)}) collective-permute-start(f32[2,136,256]{2,1,0:T(8,128)} %pad_maximum_fusion.3), channel_id=1, source_target_pairs={{0,16},{4,20},{8,24},{12,28},{1,17},{5,21},{9,25},{13,29},{2,18},{... | collective-permute-start | bytes 835592 | tf_op jit(solution)/shard_map/ppermute | solution.py:35
  90.4 0.9 reduce_window_max.31
  91.9 2.9 copy.53
  94.8 1.5 constant_dynamic-slice_fusion.9
  96.3 3.8 %collective-permute-done.3 = f32[2,136,256]{2,1,0:T(8,128)} collective-permute-done((f32[2,136,256]{2,1,0:T(8,128)}, f32[2,136,256]{2,1,0:T(8,128)}, u32[]{:S(2)}, u32[]{:S(2)}) %collective-permute-start.3) | collective-permute-done | bytes 278560 | tf_op jit(solution)/shard_map/ppermute | solution.py:35
  101.1 1.5 subtract_exponential_fusion
  102.6 1.8 fusion.17.refs_6_
  104.4 9.2 %cell.1 = bf16[1024,512]{1,0:T(8,128)(2,1)} custom-call(bf16[1024,256]{1,0:T(8,128)(2,1)} %refs_0_.1, bf16[1024,256]{1,0:T(8,128)(2,1)} %refs_1_.1, bf16[1024,512]{1,0:T(8,128)(2,1)} %refs_2_.1, f32[2,1,1024]{2,1,0:T(1,128)} %broadcast_in_dim.25.refs_3_, f32[2,1024,1]{2,1,0:T(8,128)} %get-tuple-element.133.refs_4_, ...), custom_call_target="tpu_custom_call" | custom-call | flops 4294967296 | bytes 3145728 | tf_op jit(solution)/shard_map/cell/pallas_call | solution.py:73
  113.6 4.0 %convolution_convert_fusion.2 = bf16[1024,1024]{1,0:T(8,128)(2,1)} fusion(bf16[1024,512]{1,0:T(8,128)(2,1)} %cell.1, bf16[512,1024]{0,1:T(8,128)(2,1)S(1)} %bitcast.82), kind=kOutput, calls=%fused_computation.17 | convolution fusion | flops 1074790400 | bytes 4194304 | tf_op jit(solution)/shard_map/dot_general | solution.py:116
  117.6 1.3 convolution_convert_fusion.3
  119.1 1.3 copy.65
  120.4 1.7 collective-permute-done.4
  122.1 3.3 reshape.527
  125.4 5.7 %constant_dynamic-slice_fusion.8 = (bf16[1024,1,512]{2,1,0:T(2,128)(2,1)}, bf16[1024,1,512]{2,1,0:T(2,128)(2,1)S(1)}) fusion(bf16[1024,2,512]{2,1,0:T(2,128)(2,1)S(1)} %reshape.527, s32[]{:T(128)S(6)} %select_n.269, s32[]{:T(128)S(6)} %select_n.272), kind=kLoop, calls=%fused_computation.72 | loop fusion | bytes 4194312 | tf_op jit(solution)/shard_map/jit(dynamic_index_in_dim)/dynamic_slice | solution.py:105
  131.1 1.4 fusion.11
  132.5 1.1 collective-permute-start.5
  133.7 1.4 copy.63
  135.1 23.0 %collective-permute-done.5 = bf16[1024,512]{1,0:T(8,128)(2,1)} collective-permute-done((bf16[1024,512]{1,0:T(8,128)(2,1)}, bf16[1024,512]{1,0:T(8,128)(2,1)}, u32[]{:S(2)}, u32[]{:S(2)}) %collective-permute-start.5) | collective-permute-done | bytes 1048608 | tf_op jit(solution)/shard_map/ppermute | solution.py:129
  158.0 2.5 broadcast_in_dim.30
  160.6 2.9 constant_dynamic-update-slice_fusion.3
  163.5 1.1 collective-permute-start.7
  164.6 23.2 %collective-permute-done.7 = bf16[1024,512]{1,0:T(8,128)(2,1)S(1)} collective-permute-done((bf16[1024,512]{1,0:T(8,128)(2,1)S(1)}, bf16[1024,512]{1,0:T(8,128)(2,1)S(1)}, u32[]{:S(2)}, u32[]{:S(2)}) %collective-permute-start.7) | collective-permute-done | bytes 1048608 | tf_op jit(solution)/shard_map/ppermute | solution.py:142
  187.9 2.3 constant_dynamic-update-slice_fusion.2
  190.2 1.1 constant_dynamic-update-slice_fusion.1
  191.2 1.1 constant_dynamic-update-slice_fusion
  192.3 3.1 fusion
  195.5 4.7 %constant_dynamic-slice_fusion.3 = (bf16[1408,2,1,512]{0,3,2,1:T(8,128)(2,1)}, bf16[1408,2,1,512]{0,3,2,1:T(8,128)(2,1)S(1)}) fusion(bf16[1408,2,2,512]{0,3,2,1:T(8,128)(2,1)} %bitcast.75, s32[]{:T(128)S(6)} %select_n.270, s32[]{:T(128)S(6)} %select_n.267), kind=kLoop, calls=%fused_computation.63 | loop fusion | bytes 11534344 | tf_op jit(solution)/shard_map/jit(dynamic_index_in_dim)/dynamic_slice | solution.py:115
  200.2 17.9 %all-gather.4.cloned.1.call-done = bf16[2048,1408]{1,0:T(8,128)(2,1)} async-done(((bf16[256,1408]{1,0:T(8,128)(2,1)}), bf16[2048,1408]{1,0:T(8,128)(2,1)}) %all-gather.4.cloned.1.call-update) | async-done | bytes 5767184 | tf_op jit(solution)/shard_map/all_gather | solution.py:167
  218.1 12.0 %fusion.9 = f32[1024,1408]{1,0:T(8,128)} fusion(bf16[2048,1408]{1,0:T(8,128)(2,1)} %all-gather.4.cloned.1.call-done, bf16[1024,2048]{1,0:T(8,128)(2,1)} %constant_dynamic-update-slice_fusion, f32[2048]{0:T(1024)S(1)} %convert_element_type.119, f32[1024]{0:T(1024)S(1)} %add_rsqrt_fusion), kind=kOutput, calls=%fused_computation.19 | convolution fusion | flops 5913968640 | bytes 15740928 | tf_op jit(solution)/shard_map/dot_general | solution.py:212
  230.1 80.7 %all-gather.6.cloned.1.call-done = bf16[2048,1408]{1,0:T(8,128)(2,1)} async-done(((bf16[256,1408]{1,0:T(8,128)(2,1)}), bf16[2048,1408]{1,0:T(8,128)(2,1)}) %all-gather.6.cloned.1.call-update) | async-done | bytes 5767184 | tf_op jit(solution)/shard_map/all_gather | solution.py:168
  310.8 11.5 %multiply_convert_fusion = bf16[1024,1408]{1,0:T(8,128)(2,1)S(1)} fusion(f32[1024,1408]{1,0:T(8,128)} %fusion.9, bf16[2048,1408]{1,0:T(8,128)(2,1)} %all-gather.6.cloned.1.call-done, bf16[1024,2048]{1,0:T(8,128)(2,1)} %constant_dynamic-update-slice_fusion, f32[2048]{0:T(1024)S(1)} %convert_element_type.119, f32[1024]{0:T(1024)S(1)} %add_rsqrt_fusion), kind=kOutput, calls=%fused_computation.5 | convolution fusion | flops 5922619392 | bytes 18624512 | tf_op jit(solution)/shard_map/dot_general | solution.py:213
  322.3 4.7 %convolution_convert_fusion = bf16[1024,1024]{1,0:T(8,128)(2,1)} fusion(bf16[1024,1408]{1,0:T(8,128)(2,1)S(1)} %multiply_convert_fusion, bf16[1408,1024]{0,1:T(8,128)(2,1)S(1)} %bitcast.77), kind=kOutput, calls=%fused_computation.15 | convolution fusion | flops 2953838592 | bytes 7864320 | tf_op jit(solution)/shard_map/dot_general | solution.py:116
  327.0 3.7 convolution_convert_fusion.1
  330.9 1.3 copy.69
  332.2 3.6 reshape.532
  335.8 5.7 %constant_dynamic-slice_fusion.2 = (bf16[1024,1,512]{2,1,0:T(2,128)(2,1)}, bf16[1024,1,512]{2,1,0:T(2,128)(2,1)S(1)}) fusion(bf16[1024,2,512]{2,1,0:T(2,128)(2,1)S(1)} %reshape.532, s32[]{:T(128)S(6)} %select_n.269, s32[]{:T(128)S(6)} %select_n.272), kind=kLoop, calls=%fused_computation.62 | loop fusion | bytes 4194312 | tf_op jit(solution)/shard_map/jit(dynamic_index_in_dim)/dynamic_slice | solution.py:105
  341.5 1.4 fusion.12
  342.9 1.5 collective-permute-start.10
  344.4 1.3 copy.67
  345.7 23.1 %collective-permute-done.10 = bf16[1024,512]{1,0:T(8,128)(2,1)} collective-permute-done((bf16[1024,512]{1,0:T(8,128)(2,1)}, bf16[1024,512]{1,0:T(8,128)(2,1)}, u32[]{:S(2)}, u32[]{:S(2)}) %collective-permute-start.10) | collective-permute-done | bytes 1048608 | tf_op jit(solution)/shard_map/ppermute | solution.py:129
  368.8 3.5 fusion.5
  (114 shorter events, 8.9 us)
Async XLA Ops:
  6.5 3.3 copy-start.15
  6.5 3.3 copy-start.14
  6.5 4.4 %copy-start.16 = (bf16[2,1024]{1,0:T(2,128)(2,1)S(1)}, bf16[2,1024]{1,0:T(2,128)(2,1)}, u32[]{:S(2)}) copy-start(bf16[2,1024]{1,0:T(2,128)(2,1)} %param.34) | copy-start | bytes 12292
  6.5 5.7 %copy-start.11 = (bf16[1024,256]{1,0:T(8,128)(2,1)S(1)}, bf16[1024,256]{1,0:T(8,128)(2,1)}, u32[]{:S(2)}) copy-start(bf16[1024,256]{1,0:T(8,128)(2,1)} %refs_1_.1) | copy-start | bytes 1572868
  6.5 6.3 %copy-start.19 = (bf16[1024,512]{1,0:T(8,128)(2,1)S(1)}, bf16[1024,512]{1,0:T(8,128)(2,1)}, u32[]{:S(2)}) copy-start(bf16[1024,512]{1,0:T(8,128)(2,1)} %refs_2_.1) | copy-start | bytes 3145732
  6.6 188.9 %all-gather.8.cloned.1.call-start = ((), (), s32[]{:S(2)}) async-start(), calls=%async_computation.2 | async-start | bytes 6488064 | tf_op jit(solution)/shard_map/all_gather | solution.py:169
  9.1 209.0 %all-gather.4.cloned.1.call-start = ((), (), s32[]{:S(2)}) async-start(), calls=%async_computation | async-start | bytes 6488064 | tf_op jit(solution)/shard_map/all_gather | solution.py:167
  9.8 301.0 %all-gather.6.cloned.1.call-start = ((), (), s32[]{:S(2)}) async-start(), calls=%async_computation.1 | async-start | bytes 6488064 | tf_op jit(solution)/shard_map/all_gather | solution.py:168
  13.3 15.1 %collective-permute-start = (f32[2,136,256]{2,1,0:T(8,128)S(1)}, f32[2,136,256]{2,1,0:T(8,128)S(1)}, u32[]{:S(2)}, u32[]{:S(2)}) collective-permute-start(f32[2,136,256]{2,1,0:T(8,128)S(1)} %pad_maximum_fusion), channel_id=1, source_target_pairs={{0,4},{4,8},{8,12},{12,16},{16,20},{20,24},{24,28},{1,5},{5,9},{9,... | collective-permute-start | bytes 835592 | tf_op jit(solution)/shard_map/ppermute | solution.py:31
  18.3 73.0 %copy-start.18 = (bf16[512]{0:T(512)(128)(2,1)S(1)}, bf16[512]{0:T(512)(128)(2,1)}, u32[]{:S(2)}) copy-start(bf16[512]{0:T(512)(128)(2,1)} %param.38) | copy-start | bytes 3076
  28.4 61.9 %copy-start.10 = (f32[2,136,256]{2,1,0:T(8,128)}, f32[2,136,256]{2,1,0:T(8,128)S(1)}, u32[]{:S(2)}) copy-start(f32[2,136,256]{2,1,0:T(8,128)S(1)} %collective-permute-done) | copy-start | bytes 835588
  28.8 9.1 %collective-permute-start.1 = (f32[2,136,256]{2,1,0:T(8,128)S(1)}, f32[2,136,256]{2,1,0:T(8,128)S(1)}, u32[]{:S(2)}, u32[]{:S(2)}) collective-permute-start(f32[2,136,256]{2,1,0:T(8,128)S(1)} %pad_maximum_fusion.1), channel_id=1, source_target_pairs={{0,4},{4,8},{8,12},{12,16},{16,20},{20,24},{24,28},{1,5},{5,9},{9,... | collective-permute-start | bytes 835592 | tf_op jit(solution)/shard_map/ppermute | solution.py:35
  37.8 52.5 %copy-start.12 = (f32[2,136,256]{2,1,0:T(8,128)}, f32[2,136,256]{2,1,0:T(8,128)S(1)}, u32[]{:S(2)}) copy-start(f32[2,136,256]{2,1,0:T(8,128)S(1)} %collective-permute-done.1) | copy-start | bytes 835588
  38.3 16.7 %collective-permute-start.2 = (f32[2,136,256]{2,1,0:T(8,128)S(1)}, f32[2,136,256]{2,1,0:T(8,128)S(1)}, u32[]{:S(2)}, u32[]{:S(2)}) collective-permute-start(f32[2,136,256]{2,1,0:T(8,128)S(1)} %pad_maximum_fusion.2), channel_id=1, source_target_pairs={{0,8},{4,12},{8,16},{12,20},{16,24},{20,28},{1,9},{5,13},{9,17},{1... | collective-permute-start | bytes 835592 | tf_op jit(solution)/shard_map/ppermute | solution.py:35
  55.0 37.0 %copy-start.13 = (f32[2,136,256]{2,1,0:T(8,128)}, f32[2,136,256]{2,1,0:T(8,128)S(1)}, u32[]{:S(2)}) copy-start(f32[2,136,256]{2,1,0:T(8,128)S(1)} %collective-permute-done.2) | copy-start | bytes 835588
  56.2 43.9 %collective-permute-start.3 = (f32[2,136,256]{2,1,0:T(8,128)}, f32[2,136,256]{2,1,0:T(8,128)}, u32[]{:S(2)}, u32[]{:S(2)}) collective-permute-start(f32[2,136,256]{2,1,0:T(8,128)} %pad_maximum_fusion.3), channel_id=1, source_target_pairs={{0,16},{4,20},{8,24},{12,28},{1,17},{5,21},{9,25},{13,29},{2,18},{... | collective-permute-start | bytes 835592 | tf_op jit(solution)/shard_map/ppermute | solution.py:35
  104.4 9.2 %copy-start.8 = (bf16[512,2,1,512]{0,3,2,1:T(8,128)(2,1)S(1)}, bf16[512,2,1,512]{0,3,2,1:T(8,128)(2,1)}, u32[]{:S(2)}) copy-start(bf16[512,2,1,512]{0,3,2,1:T(8,128)(2,1)} %get-tuple-element.130) | copy-start | bytes 3145732
  113.6 4.0 %copy-start.7 = (bf16[512,2,1,512]{0,3,2,1:T(8,128)(2,1)S(1)}, bf16[512,2,1,512]{0,3,2,1:T(8,128)(2,1)}, u32[]{:S(2)}) copy-start(bf16[512,2,1,512]{0,3,2,1:T(8,128)(2,1)} %get-tuple-element.131) | copy-start | bytes 3145732
  113.6 4.0 %copy-start.20 = (bf16[1024,512]{1,0:T(8,128)(2,1)S(1)}, bf16[1024,512]{1,0:T(8,128)(2,1)}, u32[]{:S(2)}) copy-start(bf16[1024,512]{1,0:T(8,128)(2,1)} %cell.1) | copy-start | bytes 3145732
  117.6 4.5 %collective-permute-start.4 = (bf16[1024,1024]{1,0:T(8,128)(2,1)}, bf16[1024,1024]{1,0:T(8,128)(2,1)}, u32[]{:S(2)}, u32[]{:S(2)}) collective-permute-start(bf16[1024,1024]{1,0:T(8,128)(2,1)} %convolution_convert_fusion.2), channel_id=1, source_target_pairs={{0,1},{1,0},{2,3},{3,2},{4,5},{5,4},{6,7},{7,6},{8,9},{9,8},{10,11... | collective-permute-start | bytes 6291464 | tf_op jit(solution)/shard_map/ppermute | solution.py:121
  125.4 5.7 %copy-start.3 = (bf16[1024,1,512]{2,0,1:T(8,128)(2,1)S(1)}, bf16[1024,1,512]{2,0,1:T(8,128)(2,1)}, u32[]{:S(2)}) copy-start(bf16[1024,1,512]{2,0,1:T(8,128)(2,1)} %copy.65) | copy-start | bytes 3145732
  132.5 25.5 %collective-permute-start.5 = (bf16[1024,512]{1,0:T(8,128)(2,1)}, bf16[1024,512]{1,0:T(8,128)(2,1)}, u32[]{:S(2)}, u32[]{:S(2)}) collective-permute-start(bf16[1024,512]{1,0:T(8,128)(2,1)} %fusion.11), channel_id=1, source_target_pairs={{0,2},{1,3},{2,0},{3,1},{4,6},{5,7},{6,4},{7,5},{8,10},{9,11},{10,... | collective-permute-start | bytes 3145736 | tf_op jit(solution)/shard_map/ppermute | solution.py:129
  133.7 26.9 %copy-start.1 = (bf16[1024,1,512]{2,1,0:T(2,128)(2,1)S(1)}, bf16[1024,1,512]{2,1,0:T(2,128)(2,1)}, u32[]{:S(2)}) copy-start(bf16[1024,1,512]{2,1,0:T(2,128)(2,1)} %get-tuple-element.128) | copy-start | bytes 3145732
  135.0 25.5 %copy-start.4 = (bf16[1024,1,512]{2,0,1:T(8,128)(2,1)S(1)}, bf16[1024,1,512]{2,0,1:T(8,128)(2,1)}, u32[]{:S(2)}) copy-start(bf16[1024,1,512]{2,0,1:T(8,128)(2,1)} %copy.63) | copy-start | bytes 3145732
  135.1 25.5 %copy-start.9 = (bf16[1024,512]{1,0:T(8,128)(2,1)S(1)}, bf16[1024,512]{1,0:T(8,128)(2,1)}, u32[]{:S(2)}) copy-start(bf16[1024,512]{1,0:T(8,128)(2,1)} %param.37) | copy-start | bytes 3145732
  160.5 27.3 %copy-start.17 = (bf16[2048]{0:T(1024)(128)(2,1)S(1)}, bf16[2048]{0:T(1024)(128)(2,1)}, u32[]{:S(2)}) copy-start(bf16[2048]{0:T(1024)(128)(2,1)} %param.40) | copy-start | bytes 12292
  163.5 28.9 %copy-start.5 = (bf16[1024,512]{1,0:T(8,128)(2,1)}, bf16[1024,512]{1,0:T(8,128)(2,1)S(1)}, u32[]{:S(2)}) copy-start(bf16[1024,512]{1,0:T(8,128)(2,1)S(1)} %get-tuple-element.117) | copy-start | bytes 3145732
  163.5 24.3 %collective-permute-start.7 = (bf16[1024,512]{1,0:T(8,128)(2,1)S(1)}, bf16[1024,512]{1,0:T(8,128)(2,1)S(1)}, u32[]{:S(2)}, u32[]{:S(2)}) collective-permute-start(bf16[1024,512]{1,0:T(8,128)(2,1)S(1)} %get-tuple-element.117), channel_id=1, source_target_pairs={{0,2},{1,3},{2,0},{3,1},{4,6},{5,7},{6,4},{7,5},{8,10},{9,11},{10,... | collective-permute-start | bytes 3145736 | tf_op jit(solution)/shard_map/ppermute | solution.py:142
  164.6 23.2 %collective-permute-start.6 = (bf16[1024,512]{1,0:T(8,128)(2,1)S(1)}, bf16[1024,512]{1,0:T(8,128)(2,1)}, u32[]{:S(2)}, u32[]{:S(2)}) collective-permute-start(bf16[1024,512]{1,0:T(8,128)(2,1)S(1)} %get-tuple-element.117), channel_id=1, source_target_pairs={{0,1},{1,0},{2,3},{3,2},{4,5},{5,4},{6,7},{7,6},{8,9},{9,8},{10,11... | collective-permute-start | bytes 3145736 | tf_op jit(solution)/shard_map/ppermute | solution.py:145
  187.8 3.4 collective-permute-start.8
  310.8 11.5 %copy-start.6 = (bf16[1408,2,1,512]{0,3,2,1:T(8,128)(2,1)S(1)}, bf16[1408,2,1,512]{0,3,2,1:T(8,128)(2,1)}, u32[]{:S(2)}) copy-start(bf16[1408,2,1,512]{0,3,2,1:T(8,128)(2,1)} %get-tuple-element.120) | copy-start | bytes 8650756
  327.0 5.2 %collective-permute-start.9 = (bf16[1024,1024]{1,0:T(8,128)(2,1)}, bf16[1024,1024]{1,0:T(8,128)(2,1)}, u32[]{:S(2)}, u32[]{:S(2)}) collective-permute-start(bf16[1024,1024]{1,0:T(8,128)(2,1)} %convolution_convert_fusion), channel_id=1, source_target_pairs={{0,1},{1,0},{2,3},{3,2},{4,5},{5,4},{6,7},{7,6},{8,9},{9,8},{10,11... | collective-permute-start | bytes 6291464 | tf_op jit(solution)/shard_map/ppermute | solution.py:121
  335.8 5.7 %copy-start.2 = (bf16[1024,1,512]{2,0,1:T(8,128)(2,1)S(1)}, bf16[1024,1,512]{2,0,1:T(8,128)(2,1)}, u32[]{:S(2)}) copy-start(bf16[1024,1,512]{2,0,1:T(8,128)(2,1)} %copy.69) | copy-start | bytes 3145732
  341.5 27.3 %copy-start = (bf16[1024,1,512]{2,1,0:T(2,128)(2,1)S(1)}, bf16[1024,1,512]{2,1,0:T(2,128)(2,1)}, u32[]{:S(2)}) copy-start(bf16[1024,1,512]{2,1,0:T(2,128)(2,1)} %get-tuple-element.122) | copy-start | bytes 3145732
  342.9 25.9 %collective-permute-start.10 = (bf16[1024,512]{1,0:T(8,128)(2,1)}, bf16[1024,512]{1,0:T(8,128)(2,1)}, u32[]{:S(2)}, u32[]{:S(2)}) collective-permute-start(bf16[1024,512]{1,0:T(8,128)(2,1)} %fusion.12), channel_id=1, source_target_pairs={{0,2},{1,3},{2,0},{3,1},{4,6},{5,7},{6,4},{7,5},{8,10},{9,11},{10,... | collective-permute-start | bytes 3145736 | tf_op jit(solution)/shard_map/ppermute | solution.py:129
Sparse Core Ops, SparseCore 0:
  9.5 104.4 all-gather.7
  116.2 101.8 all-gather.3
  220.3 90.4 all-gather.5

commit v2 on v1

--- a/solution.py
+++ b/solution.py
@@ -101,34 +101,27 @@
     return [(i, (i + 2 * step) % count) for i in range(count)]
 
 
-def take(array, index):
-    return lax.dynamic_index_in_dim(array, index, 1, keepdims=False)
-
-
 def product_scattered(rows, weight):
     count, index = lax.axis_size("tp"), lax.axis_index("tp")
     chips, core, chip = count // 2, index % 2, index // 2
     width = weight.shape[1] // count
-    split = weight.reshape(weight.shape[0], chips, 2, width)
-
-    def half(which):
-        chosen = lax.dynamic_index_in_dim(split, which, 2, keepdims=False)
-        return jnp.dot(
-            rows, chosen.reshape(weight.shape[0], chips * width), preferred_element_type=jnp.float32
-        )
-
-    given = half(1 - core).astype(jnp.bfloat16)
-    got = lax.ppermute(given, "tp", partner_pairs(count))
-    kept = half(core).astype(jnp.bfloat16)
-    shape = (rows.shape[0], chips, width)
-    kept, got = kept.reshape(shape), got.reshape(shape)
-    total = take(kept, chip).astype(jnp.float32) + take(got, chip).astype(jnp.float32)
+
+    def product(block):
+        columns = lax.dynamic_slice_in_dim(weight, block * width, width, 1)
+        return jnp.dot(rows, columns, preferred_element_type=jnp.float32)
+
+    def chip_sum(to):
+        given = product(2 * to + 1 - core).astype(jnp.bfloat16)
+        got = lax.ppermute(given, "tp", partner_pairs(count))
+        return product(2 * to + core) + got.astype(jnp.float32)
+
+    moved = []
     for step in range(1, chips):
-        to = (chip + step) % chips
-        sent = take(kept, to).astype(jnp.float32) + take(got, to).astype(jnp.float32)
-        total = total + lax.ppermute(
-            sent.astype(jnp.bfloat16), "tp", ring_pairs(count, step)
-        ).astype(jnp.float32)
+        sent = chip_sum((chip + step) % chips).astype(jnp.bfloat16)
+        moved.append(lax.ppermute(sent, "tp", ring_pairs(count, step)))
+    total = chip_sum(chip)
+    for part in moved:
+        total = total + part.astype(jnp.float32)
     return total
 
 
@@ -166,7 +159,6 @@
 ):
     whole_gate = lax.all_gather(gate_projection_weight, "sp", axis=0, tiled=True)
     whole_up = lax.all_gather(up_projection_weight, "sp", axis=0, tiled=True)
-    whole_down = lax.all_gather(down_projection_weight, "sp", axis=1, tiled=True)
     length = queries.shape[0]
     heads = input_gate_logits.shape[0]
     dk, dv = queries.shape[1] // heads, cell_value_rows.shape[1] // heads
@@ -206,6 +198,8 @@
     )
     summed = product_scattered(gated, cell_output_weight)
     stream = (residual.astype(jnp.float32) + summed).astype(jnp.bfloat16)
+    down_late, stream = lax.optimization_barrier((down_projection_weight, stream))
+    whole_down = lax.all_gather(down_late, "sp", axis=1, tiled=True)
     wide = columns_gathered(stream).astype(jnp.float32)
     scale = lax.rsqrt(jnp.mean(wide * wide, axis=-1, keepdims=True) + EPSILON)
     normed = (wide * scale * feedforward_norm_gain.astype(jnp.float32)[None, :]).astype(jnp.bfloat16)

time: 380 us -> 358 us (0.942)
  local copies, waits for them, and re-layouts: 45.9 us -> 9.38 us
  waiting for transfers between devices: 192 us -> 203 us
  matrix products: 37.6 us -> 46.1 us
  other arithmetic: 20.3 us -> 15.9 us
    all_gather x1, waiting for transfers between devices: 0.02 us -> 81 us  [local(): whole_down = lax.all_gather(down_late, 'sp', axis=1, tiled=True)]
    all_gather x1, waiting for transfers between devices: 80.7 us -> 24.3 us  [local(): whole_up = lax.all_gather(up_projection_weight, 'sp', axis=0, tiled=True)]
    dynamic_slice x6 -> x0, local copies, waits for them, and re-layouts: 18 us -> none  [the longest x4 11.7 us: take(): return lax.dynamic_index_in_dim(array, index, 1, keepdims=False)]
    all_gather x1, waiting for transfers between devices: 17.9 us -> 0.02 us  [local(): lax.all_gather(gate_projection_weight, 'sp', axis=0, tiled=True)]
    unnamed x51 -> x25, local copies, waits for them, and re-layouts: 11 us -> 3.9 us
    reshape x2 -> x0, local copies, waits for them, and re-layouts: 6.87 us -> none  [product_scattered(): kept, got = (kept.reshape(shape), got.reshape(shape))]
    dot_general x4 -> x8, matrix products: 13.7 us -> 19.1 us  [product(): return jnp.dot(rows, columns, preferred_element_type=jnp.float32)]
    ppermute x3, waiting for transfers between devices: 11.8 us -> 15.8 us  [entering_state(): moved = lax.ppermute(pack(s, t, f), 'sp', shift_pairs(length, step))]
  transfers between devices with their start and end apart: 14 -> 16, of which waited for: 10 -> 11; matrix products, arithmetic and copies ran while one was open for 19% -> 18% of each run, Pallas kernels for 2% -> 3%
where the time goes in v2:
time: 358 us; the launch traced here: 357 us
  waiting for transfers between devices  203 us (57%)
  starting transfers between devices  59.9 us (17%)
  matrix products  46.1 us (13%)
  other arithmetic  15.9 us (4%)
  between operations  13.5 us (4%)
  local copies, waits for them, and re-layouts  9.38 us (3%)
  Pallas kernels  9.13 us (3%)
    all_gather x1, waiting for transfers between devices, local(): whole_down = lax.all_gather(down_late, 'sp', axis=1, tiled=True)  81 us
    ppermute x3, starting transfers between devices, entering_state(): moved = lax.ppermute(pack(s, t, f), 'sp', shift_pairs(length, step))  48.6 us
    ppermute x2, waiting for transfers between devices, product_scattered(): moved.append(lax.ppermute(sent, 'tp', ring_pairs(count, step)))  45 us
    all_gather x1, waiting for transfers between devices, local(): whole_up = lax.all_gather(up_projection_weight, 'sp', axis=0, tiled=True)  24.3 us
    ppermute x1, waiting for transfers between devices, columns_gathered(): moved = lax.ppermute(block, 'tp', ring_pairs(count, step))  22.8 us
    dot_general x8, matrix products, product(): return jnp.dot(rows, columns, preferred_element_type=jnp.float32)  19.1 us
    ppermute x3, waiting for transfers between devices, entering_state(): moved = lax.ppermute(pack(s, t, f), 'sp', shift_pairs(length, step))  15.8 us
    dot_general x1, matrix products, local(): lifted = jnp.dot(normed, whole_up, preferred_element_type=jnp.float32)  12.4 us
  transfers between devices with their start and end apart: 16, of which 11 were waited for; matrix products, arithmetic and copies ran while one was open for 18% of the time, Pallas kernels for 3%

profile of v2, /device:TPU:0, one launch (start us, length us, event | category | flops | bytes accessed | tf_op | source)
XLA Modules:
  0.0 357.1 jit_solution(13519535385364474644)
XLA Ops:
  6.5 0.7 all-gather.4.cloned.1.call-update
  7.3 0.7 all-gather.6.cloned.1.call-update
  8.1 0.7 fusion.33
  8.8 0.6 reduce-window.14
  9.8 0.7 convert_subtract_fusion
  11.8 1.2 copy.21
  13.4 1.3 convolution_bitcast_fusion
  14.7 1.3 convolution_bitcast_fusion.1
  16.0 4.9 %collective-permute-start = (f32[2,136,256]{2,1,0:T(8,128)S(1)}, f32[2,136,256]{2,1,0:T(8,128)S(1)}, u32[]{:S(2)}, u32[]{:S(2)}) collective-permute-start(f32[2,136,256]{2,1,0:T(8,128)S(1)} %pad_maximum_fusion), channel_id=1, source_target_pairs={{0,4},{4,8},{8,12},{12,16},{16,20},{20,24},{24,28},{1,5},{5,9},{9,... | collective-permute-start | bytes 835592 | tf_op jit(solution)/shard_map/ppermute | solution.py:31
  20.9 12.4 %collective-permute-done = f32[2,136,256]{2,1,0:T(8,128)S(1)} collective-permute-done((f32[2,136,256]{2,1,0:T(8,128)S(1)}, f32[2,136,256]{2,1,0:T(8,128)S(1)}, u32[]{:S(2)}, u32[]{:S(2)}) %collective-permute-start) | collective-permute-done | bytes 278560 | tf_op jit(solution)/shard_map/ppermute | solution.py:31
  33.6 4.4 %collective-permute-start.1 = (f32[2,136,256]{2,1,0:T(8,128)S(1)}, f32[2,136,256]{2,1,0:T(8,128)S(1)}, u32[]{:S(2)}, u32[]{:S(2)}) collective-permute-start(f32[2,136,256]{2,1,0:T(8,128)S(1)} %pad_maximum_fusion.1), channel_id=1, source_target_pairs={{0,4},{4,8},{8,12},{12,16},{16,20},{20,24},{24,28},{1,5},{5,9},{9,... | collective-permute-start | bytes 835592 | tf_op jit(solution)/shard_map/ppermute | solution.py:35
  38.1 4.9 %collective-permute-done.1 = f32[2,136,256]{2,1,0:T(8,128)S(1)} collective-permute-done((f32[2,136,256]{2,1,0:T(8,128)S(1)}, f32[2,136,256]{2,1,0:T(8,128)S(1)}, u32[]{:S(2)}, u32[]{:S(2)}) %collective-permute-start.1) | collective-permute-done | bytes 278560 | tf_op jit(solution)/shard_map/ppermute | solution.py:35
  43.4 13.5 %collective-permute-start.2 = (f32[2,136,256]{2,1,0:T(8,128)S(1)}, f32[2,136,256]{2,1,0:T(8,128)}, u32[]{:S(2)}, u32[]{:S(2)}) collective-permute-start(f32[2,136,256]{2,1,0:T(8,128)S(1)} %pad_maximum_fusion.2), channel_id=1, source_target_pairs={{0,8},{4,12},{8,16},{12,20},{16,24},{20,28},{1,9},{5,13},{9,17},{1... | collective-permute-start | bytes 835592 | tf_op jit(solution)/shard_map/ppermute | solution.py:35
  56.9 3.3 collective-permute-done.2
  60.3 0.9 fusion.48
  61.5 1.1 fusion.28
  62.6 0.7 pad_maximum_fusion.3
  63.3 30.6 %collective-permute-start.3 = (f32[2,136,256]{2,1,0:T(8,128)}, f32[2,136,256]{2,1,0:T(8,128)}, u32[]{:S(2)}, u32[]{:S(2)}) collective-permute-start(f32[2,136,256]{2,1,0:T(8,128)} %pad_maximum_fusion.3), channel_id=1, source_target_pairs={{0,16},{4,20},{8,24},{12,28},{1,17},{5,21},{9,25},{13,29},{2,18},{... | collective-permute-start | bytes 835592 | tf_op jit(solution)/shard_map/ppermute | solution.py:35
  94.0 0.6 broadcast_in_dim.25.refs_3_
  94.7 0.9 reduce_window_max.31
  96.1 7.6 %collective-permute-done.3 = f32[2,136,256]{2,1,0:T(8,128)} collective-permute-done((f32[2,136,256]{2,1,0:T(8,128)}, f32[2,136,256]{2,1,0:T(8,128)}, u32[]{:S(2)}, u32[]{:S(2)}) %collective-permute-start.3) | collective-permute-done | bytes 278560 | tf_op jit(solution)/shard_map/ppermute | solution.py:35
  103.7 0.8 add_add_fusion
  104.7 1.7 fusion.26.refs_6_
  106.5 1.5 subtract_exponential_fusion
  108.0 9.1 %cell.1 = bf16[1024,512]{1,0:T(8,128)(2,1)} custom-call(bf16[1024,256]{1,0:T(8,128)(2,1)} %refs_0_.1, bf16[1024,256]{1,0:T(8,128)(2,1)} %refs_1_.1, bf16[1024,512]{1,0:T(8,128)(2,1)} %refs_2_.1, f32[2,1,1024]{2,1,0:T(1,128)} %broadcast_in_dim.25.refs_3_, f32[2,1024,1]{2,1,0:T(8,128)} %get-tuple-element.123.refs_4_, ...), custom_call_target="tpu_custom_call" | custom-call | flops 4294967296 | bytes 3145728 | tf_op jit(solution)/shard_map/cell/pallas_call | solution.py:73
  117.1 3.0 convolution_convert_fusion.2
  120.1 3.0 convolution_convert_fusion.3
  123.6 2.9 add_convert_fusion.3
  126.5 2.3 collective-permute-start.6
  128.8 0.7 fusion.21
  129.6 22.9 %collective-permute-done.6 = bf16[1024,512]{1,0:T(8,128)(2,1)} collective-permute-done((bf16[1024,512]{1,0:T(8,128)(2,1)}, bf16[1024,512]{1,0:T(8,128)(2,1)}, u32[]{:S(2)}, u32[]{:S(2)}) %collective-permute-start.6) | collective-permute-done | bytes 1048608 | tf_op jit(solution)/shard_map/ppermute | solution.py:121
  152.5 2.2 add_convert_fusion.2
  154.7 1.8 collective-permute-start.8
  156.5 22.8 %collective-permute-done.8 = bf16[1024,512]{1,0:T(8,128)(2,1)S(1)} collective-permute-done((bf16[1024,512]{1,0:T(8,128)(2,1)S(1)}, bf16[1024,512]{1,0:T(8,128)(2,1)S(1)}, u32[]{:S(2)}, u32[]{:S(2)}) %collective-permute-start.8) | collective-permute-done | bytes 1048608 | tf_op jit(solution)/shard_map/ppermute | solution.py:135
  180.0 1.4 constant_dynamic-update-slice_fusion.2
  182.1 2.0 copy-done.2
  184.2 0.9 fusion
  185.1 12.0 %fusion.12 = f32[1024,1408]{1,0:T(8,128)} fusion(bf16[2048,1408]{1,0:T(8,128)(2,1)} %all-gather.4.cloned.1.call-done, bf16[1024,2048]{1,0:T(8,128)(2,1)} %copy-done.2, f32[2048]{0:T(1024)S(1)} %convert_element_type.90, f32[1024]{0:T(1024)S(1)} %add_rsqrt_fusion), kind=kOutput, calls=%fused_computation.20 | convolution fusion | flops 5913968640 | bytes 15740928 | tf_op jit(solution)/shard_map/dot_general | solution.py:206
  197.1 24.3 %all-gather.6.cloned.1.call-done = bf16[2048,1408]{1,0:T(8,128)(2,1)} async-done(((bf16[256,1408]{1,0:T(8,128)(2,1)}), bf16[2048,1408]{1,0:T(8,128)(2,1)}) %all-gather.6.cloned.1.call-update) | async-done | bytes 5767184 | tf_op jit(solution)/shard_map/all_gather | solution.py:161
  221.4 12.4 %multiply_convert_fusion = bf16[1024,1408]{1,0:T(8,128)(2,1)} fusion(f32[1024,1408]{1,0:T(8,128)} %fusion.12, bf16[2048,1408]{1,0:T(8,128)(2,1)} %all-gather.6.cloned.1.call-done, bf16[1024,2048]{1,0:T(8,128)(2,1)} %copy-done.2, f32[2048]{0:T(1024)S(1)} %convert_element_type.90, f32[1024]{0:T(1024)S(1)} %add_rsqrt_fusion), kind=kOutput, calls=%fused_computation.5 | convolution fusion | flops 5922619392 | bytes 18624512 | tf_op jit(solution)/shard_map/dot_general | solution.py:207
  233.8 81.0 %all-gather.8.cloned.1.call-done = bf16[1408,2048]{1,0:T(8,128)(2,1)} async-done(((bf16[1408,256]{1,0:T(8,128)(2,1)}), bf16[1408,2048]{1,0:T(8,128)(2,1)}) %all-gather.8.cloned.1.call-update) | async-done | bytes 5767184 | tf_op jit(solution)/shard_map/all_gather | solution.py:202
  314.8 4.2 %convolution_convert_fusion = bf16[1024,512]{1,0:T(8,128)(2,1)S(1)} fusion(bf16[1024,1408]{1,0:T(8,128)(2,1)} %multiply_convert_fusion, bf16[1408,2048]{1,0:T(8,128)(2,1)} %all-gather.8.cloned.1.call-done, s32[]{:T(128)S(6)} %select_n.261), kind=kOutput, calls=%fused_computation.10 | convolution fusion | flops 1476919296 | bytes 5373956 | tf_op jit(solution)/shard_map/dot_general | solution.py:111
  319.6 1.8 convolution_convert_fusion.1
  321.7 1.8 add_convert_fusion.1
  323.5 1.6 collective-permute-start.12
  325.1 1.8 fusion.7
  326.9 22.1 %collective-permute-done.12 = bf16[1024,512]{1,0:T(8,128)(2,1)S(1)} collective-permute-done((bf16[1024,512]{1,0:T(8,128)(2,1)S(1)}, bf16[1024,512]{1,0:T(8,128)(2,1)S(1)}, u32[]{:S(2)}, u32[]{:S(2)}) %collective-permute-start.12) | collective-permute-done | bytes 1048608 | tf_op jit(solution)/shard_map/ppermute | solution.py:121
  348.9 1.6 add_convert_fusion
  (87 shorter events, 6.8 us)
Async XLA Ops:
  6.5 110.6 %copy-start = (bf16[512,2048]{1,0:T(8,128)(2,1)S(1)}, bf16[512,2048]{1,0:T(8,128)(2,1)}, u32[]{:S(2)}) copy-start(bf16[512,2048]{1,0:T(8,128)(2,1)} %param.39) | copy-start | bytes 6291460
  6.5 178.5 %all-gather.4.cloned.1.call-start = ((), (), s32[]{:S(2)}) async-start(), calls=%async_computation | async-start | bytes 6488064 | tf_op jit(solution)/shard_map/all_gather | solution.py:160
  7.3 214.1 %all-gather.6.cloned.1.call-start = ((), (), s32[]{:S(2)}) async-start(), calls=%async_computation.1 | async-start | bytes 6488064 | tf_op jit(solution)/shard_map/all_gather | solution.py:161
  8.0 306.8 %all-gather.8.cloned.1.call-start = ((), (), s32[]{:S(2)}) async-start(), calls=%async_computation.2 | async-start | bytes 6488064 | tf_op jit(solution)/shard_map/all_gather | solution.py:202
  13.3 82.3 %copy-start.8 = (bf16[512]{0:T(512)(128)(2,1)S(1)}, bf16[512]{0:T(512)(128)(2,1)}, u32[]{:S(2)}) copy-start(bf16[512]{0:T(512)(128)(2,1)} %param.38) | copy-start | bytes 3076
  16.0 17.3 %collective-permute-start = (f32[2,136,256]{2,1,0:T(8,128)S(1)}, f32[2,136,256]{2,1,0:T(8,128)S(1)}, u32[]{:S(2)}, u32[]{:S(2)}) collective-permute-start(f32[2,136,256]{2,1,0:T(8,128)S(1)} %pad_maximum_fusion), channel_id=1, source_target_pairs={{0,4},{4,8},{8,12},{12,16},{16,20},{20,24},{24,28},{1,5},{5,9},{9,... | collective-permute-start | bytes 835592 | tf_op jit(solution)/shard_map/ppermute | solution.py:31
  33.3 61.3 %copy-start.5 = (f32[2,136,256]{2,1,0:T(8,128)}, f32[2,136,256]{2,1,0:T(8,128)S(1)}, u32[]{:S(2)}) copy-start(f32[2,136,256]{2,1,0:T(8,128)S(1)} %collective-permute-done) | copy-start | bytes 835588
  33.6 9.3 %collective-permute-start.1 = (f32[2,136,256]{2,1,0:T(8,128)S(1)}, f32[2,136,256]{2,1,0:T(8,128)S(1)}, u32[]{:S(2)}, u32[]{:S(2)}) collective-permute-start(f32[2,136,256]{2,1,0:T(8,128)S(1)} %pad_maximum_fusion.1), channel_id=1, source_target_pairs={{0,4},{4,8},{8,12},{12,16},{16,20},{20,24},{24,28},{1,5},{5,9},{9,... | collective-permute-start | bytes 835592 | tf_op jit(solution)/shard_map/ppermute | solution.py:35
  42.9 51.6 %copy-start.6 = (f32[2,136,256]{2,1,0:T(8,128)}, f32[2,136,256]{2,1,0:T(8,128)S(1)}, u32[]{:S(2)}) copy-start(f32[2,136,256]{2,1,0:T(8,128)S(1)} %collective-permute-done.1) | copy-start | bytes 835588
  43.4 16.9 %collective-permute-start.2 = (f32[2,136,256]{2,1,0:T(8,128)S(1)}, f32[2,136,256]{2,1,0:T(8,128)}, u32[]{:S(2)}, u32[]{:S(2)}) collective-permute-start(f32[2,136,256]{2,1,0:T(8,128)S(1)} %pad_maximum_fusion.2), channel_id=1, source_target_pairs={{0,8},{4,12},{8,16},{12,20},{16,24},{20,28},{1,9},{5,13},{9,17},{1... | collective-permute-start | bytes 835592 | tf_op jit(solution)/shard_map/ppermute | solution.py:35
  63.3 40.4 %collective-permute-start.3 = (f32[2,136,256]{2,1,0:T(8,128)}, f32[2,136,256]{2,1,0:T(8,128)}, u32[]{:S(2)}, u32[]{:S(2)}) collective-permute-start(f32[2,136,256]{2,1,0:T(8,128)} %pad_maximum_fusion.3), channel_id=1, source_target_pairs={{0,16},{4,20},{8,24},{12,28},{1,17},{5,21},{9,25},{13,29},{2,18},{... | collective-permute-start | bytes 835592 | tf_op jit(solution)/shard_map/ppermute | solution.py:35
  117.1 6.5 %copy-start.3 = (bf16[1024,512]{1,0:T(8,128)(2,1)S(1)}, bf16[1024,512]{1,0:T(8,128)(2,1)}, u32[]{:S(2)}) copy-start(bf16[1024,512]{1,0:T(8,128)(2,1)} %cell.1) | copy-start | bytes 3145732
  120.1 3.5 collective-permute-start.5
  123.1 6.4 %collective-permute-start.4 = (bf16[1024,512]{1,0:T(8,128)(2,1)}, bf16[1024,512]{1,0:T(8,128)(2,1)}, u32[]{:S(2)}, u32[]{:S(2)}) collective-permute-start(bf16[1024,512]{1,0:T(8,128)(2,1)} %convolution_convert_fusion.3), channel_id=1, source_target_pairs={{0,1},{1,0},{2,3},{3,2},{4,5},{5,4},{6,7},{7,6},{8,9},{9,8},{10,11... | collective-permute-start | bytes 3145736 | tf_op jit(solution)/shard_map/ppermute | solution.py:115
  126.5 25.9 %collective-permute-start.6 = (bf16[1024,512]{1,0:T(8,128)(2,1)}, bf16[1024,512]{1,0:T(8,128)(2,1)}, u32[]{:S(2)}, u32[]{:S(2)}) collective-permute-start(bf16[1024,512]{1,0:T(8,128)(2,1)} %add_convert_fusion.3), channel_id=1, source_target_pairs={{0,2},{1,3},{2,0},{3,1},{4,6},{5,7},{6,4},{7,5},{8,10},{9,11},{10,... | collective-permute-start | bytes 3145736 | tf_op jit(solution)/shard_map/ppermute | solution.py:121
  128.8 23.6 %copy-start.4 = (bf16[1024,512]{1,0:T(8,128)(2,1)S(1)}, bf16[1024,512]{1,0:T(8,128)(2,1)}, u32[]{:S(2)}) copy-start(bf16[1024,512]{1,0:T(8,128)(2,1)} %param.37) | copy-start | bytes 3145732
  129.5 49.8 %copy-start.7 = (bf16[2048]{0:T(1024)(128)(2,1)S(1)}, bf16[2048]{0:T(1024)(128)(2,1)}, u32[]{:S(2)}) copy-start(bf16[2048]{0:T(1024)(128)(2,1)} %param.40) | copy-start | bytes 12292
  154.7 24.6 %collective-permute-start.8 = (bf16[1024,512]{1,0:T(8,128)(2,1)S(1)}, bf16[1024,512]{1,0:T(8,128)(2,1)S(1)}, u32[]{:S(2)}, u32[]{:S(2)}) collective-permute-start(bf16[1024,512]{1,0:T(8,128)(2,1)S(1)} %add_convert_fusion.2), channel_id=1, source_target_pairs={{0,2},{1,3},{2,0},{3,1},{4,6},{5,7},{6,4},{7,5},{8,10},{9,11},{10,... | collective-permute-start | bytes 3145736 | tf_op jit(solution)/shard_map/ppermute | solution.py:135
  156.5 23.5 %collective-permute-start.7 = (bf16[1024,512]{1,0:T(8,128)(2,1)S(1)}, bf16[1024,512]{1,0:T(8,128)(2,1)}, u32[]{:S(2)}, u32[]{:S(2)}) collective-permute-start(bf16[1024,512]{1,0:T(8,128)(2,1)S(1)} %add_convert_fusion.2), channel_id=1, source_target_pairs={{0,1},{1,0},{2,3},{3,2},{4,5},{5,4},{6,7},{7,6},{8,9},{9,8},{10,11... | collective-permute-start | bytes 3145736 | tf_op jit(solution)/shard_map/ppermute | solution.py:138
  179.3 2.7 collective-permute-start.9
  182.1 2.0 copy-start.2
  314.8 4.2 %copy-start.9 = (bf16[1408,2048]{1,0:T(8,128)(2,1)S(1)}, bf16[1408,2048]{1,0:T(8,128)(2,1)}, u32[]{:S(2)}) copy-start(bf16[1408,2048]{1,0:T(8,128)(2,1)} %all-gather.8.cloned.1.call-done) | copy-start | bytes 17301508
  314.8 4.8 %copy-start.10 = (bf16[1024,1408]{1,0:T(8,128)(2,1)S(1)}, bf16[1024,1408]{1,0:T(8,128)(2,1)}, u32[]{:S(2)}) copy-start(bf16[1024,1408]{1,0:T(8,128)(2,1)} %multiply_convert_fusion) | copy-start | bytes 8650756
  319.0 2.7 collective-permute-start.11
  321.4 5.4 %collective-permute-start.10 = (bf16[1024,512]{1,0:T(8,128)(2,1)S(1)}, bf16[1024,512]{1,0:T(8,128)(2,1)S(1)}, u32[]{:S(2)}, u32[]{:S(2)}) collective-permute-start(bf16[1024,512]{1,0:T(8,128)(2,1)S(1)} %convolution_convert_fusion.1), channel_id=1, source_target_pairs={{0,1},{1,0},{2,3},{3,2},{4,5},{5,4},{6,7},{7,6},{8,9},{9,8},{10,11... | collective-permute-start | bytes 3145736 | tf_op jit(solution)/shard_map/ppermute | solution.py:115
  323.5 25.5 %collective-permute-start.12 = (bf16[1024,512]{1,0:T(8,128)(2,1)S(1)}, bf16[1024,512]{1,0:T(8,128)(2,1)S(1)}, u32[]{:S(2)}, u32[]{:S(2)}) collective-permute-start(bf16[1024,512]{1,0:T(8,128)(2,1)S(1)} %add_convert_fusion.1), channel_id=1, source_target_pairs={{0,2},{1,3},{2,0},{3,1},{4,6},{5,7},{6,4},{7,5},{8,10},{9,11},{10,... | collective-permute-start | bytes 3145736 | tf_op jit(solution)/shard_map/ppermute | solution.py:121
  325.1 25.5 %copy-start.1 = (bf16[512,2048]{1,0:T(8,128)(2,1)S(1)}, bf16[512,2048]{1,0:T(8,128)(2,1)}, u32[]{:S(2)}) copy-start(bf16[512,2048]{1,0:T(8,128)(2,1)} %param.39) | copy-start | bytes 6291460
Sparse Core Ops, SparseCore 0:
  9.5 105.0 all-gather.3
  116.8 104.5 all-gather.5
  223.4 91.3 all-gather.7
